TPU v7x, 128 devices: a whole 4x4x4 slice. The times are simulated.
128 devices in a mesh: sp: 32 (over z, y, core), tp: 4 (over x).
Axes of the slice: x: 4, y: 4, z: 4, core: 2. Of those that a mesh axis runs over, the one named last changes fastest.
Arguments:
- residual_in: bfloat16 [32768, 2048], P(('sp', 'tp')), may hold values from -6 to 6
- queries: bfloat16 [32768, 2048], P('sp', 'tp'), may hold values from -200 to 200, as said below
- keys_values: bfloat16 [2, 32768, 1024], P(None, 'sp', 'tp'), may hold values from -6 to 6
- sink_logit: float32 [32], P('tp'), may hold values from -2 to 6
- out_weight: bfloat16 [2048, 2048], P('tp'), may hold values from -2 to 2
- norm1_gain: float32 [2048], replicated, may hold values from 0.1 to 1.9
- norm1_bias: float32 [2048], replicated, may hold values from -3 to 3
- up_weight: bfloat16 [2048, 8192], P('sp', 'tp'), may hold values from -0.125 to 0.125
- down_weight: bfloat16 [8192, 2048], P('tp', 'sp'), may hold values from -0.0625 to 0.0625
- norm2_gain: float32 [2048], replicated, may hold values from 0.1 to 1.9
- norm2_bias: float32 [2048], replicated, may hold values from -3 to 3
Outputs:
- stream_out: bfloat16 [32768, 2048], P(('sp', 'tp'))
Inputs may be any that keep to these rules, and one draw needn't show every extreme that they name: `queries`: of order one mostly; some rows may be large multiples of a nearby key row.
All inputs are finite; a program needn't handle non-finite values.
Results may differ from a plain program's by a relative error of at most 0.014.
Values may be sent and summed in bfloat16 or wider, within the bound.
A program may use at most 128 MiB of HBM per device.

v0:
```python
import functools

import jax
import jax.numpy as jnp
from jax import lax
from jax.experimental import pallas as pl
from jax.experimental.pallas import tpu as pltpu
from jax.sharding import PartitionSpec as P

HEAD_DIM = 64
WINDOW = 128
BLOCK = 128
MESH = pl.DeviceIdType.MESH
F32 = jnp.float32
BF16 = jnp.bfloat16
ALL = slice(None)


def norm_rows(values, gain, bias):
    mean = jnp.mean(values, axis=-1, keepdims=True)
    centred = values - mean
    variance = jnp.mean(centred * centred, axis=-1, keepdims=True)
    return (centred * lax.rsqrt(variance + 1e-06) * gain + bias).astype(BF16)


def aligned(index, size):
    return pl.multiple_of(index * size, size)


class Links:
    def __init__(self, send, recv):
        self.send, self.recv, self.count, self.started = send, recv, 0, []

    def take(self):
        self.count += 1
        return self.count - 1

    def copy(self, src, dst, ident, target):
        return pltpu.make_async_remote_copy(
            src_ref=src,
            dst_ref=dst,
            send_sem=self.send.at[ident],
            recv_sem=self.recv.at[ident],
            device_id=target,
            device_id_type=MESH,
        )

    def start(self, src, dst, ident, target, again=None):
        self.copy(src, dst, ident, target).start()
        self.started.append((again or (lambda: src), ident, target))

    def arrived(self, dst, ident, target):
        self.copy(dst, dst, ident, target).wait_recv()

    def finish(self):
        for again, ident, target in self.started:
            src = again()
            self.copy(src, src, ident, target).wait_send()


class Spread:
    def __init__(self, links, part, first, second, core, peers, sister):
        self.links, self.part, self.core, self.sister = links, part, core, sister
        self.own1, self.own2 = first, second
        self.up1, self.down1, self.up2, self.down2 = peers
        self.ids = [links.take() for _ in range(12)]
        self.near1 = [(first + hop) % 4 for hop in (3, 1, 2)]
        self.near2 = [(second + hop) % 4 for hop in (3, 1, 2)]

    def at(self, one, two, sub=None, core=None):
        return self.part(one, two, self.core if core is None else core, sub)

    def push(self, ident, target, one, two, sub=None, source=None):
        place = self.at(one, two, sub)
        again = (lambda: self.at(one, two, sub)) if source is None else (lambda: source)
        src = place if source is None else source
        self.links.start(src, place, self.ids[ident], target, again)

    def pull(self, ident, target, one, two, sub=None, core=None):
        self.links.arrived(self.at(one, two, sub, core), self.ids[ident], target)

    def step1(self):
        self.push(0, self.up1, self.own1, self.own2)
        self.push(1, self.down1, self.own1, self.own2)

    def step2(self):
        before, after, _ = self.near1
        self.pull(0, self.up1, before, self.own2)
        self.push(2, self.up1, before, self.own2, 0)
        self.pull(1, self.down1, after, self.own2)
        self.push(3, self.down1, after, self.own2, 1)

    def step3(self):
        across = self.near1[2]
        self.pull(2, self.up1, across, self.own2, 0)
        self.pull(3, self.down1, across, self.own2, 1)
        self.push(4, self.up2, ALL, self.own2)
        self.push(5, self.down2, ALL, self.own2)
        self.push(8, self.sister, ALL, self.own2)

    def step4(self):
        before, after, _ = self.near2
        self.pull(4, self.up2, ALL, before)
        self.push(6, self.up2, ALL, before, 0)
        self.pull(5, self.down2, ALL, after)
        self.push(7, self.down2, ALL, after, 1)
        self.push(9, self.sister, ALL, before)
        self.push(10, self.sister, ALL, after)

    def step5(self):
        across = self.near2[2]
        self.pull(6, self.up2, ALL, across, 0)
        self.pull(7, self.down2, ALL, across, 1)
        self.push(11, self.sister, ALL, across)

    def step6(self):
        for place, ident in zip([self.own2] + self.near2, (8, 9, 10, 11)):
            self.pull(ident, self.sister, ALL, place, None, 1 - self.core)


def layer_kernel(
    total, res_h, q_h, kv_h, sink_ref, ow_h, g1_ref, b1_ref, up_h, dn_h, g2_ref, b2_ref, out_h,
    qv, kvv, att, attr, resv, oww, upw, dnw, raw, slab, rows, act, pre, part, own, rin, rfin, outv,
    local, send, recv, asend, arecv,
):
    sp, x = lax.axis_index("sp"), lax.axis_index("tp")
    core, chip = sp % 2, sp // 2
    y, z = chip % 4, chip // 4

    def device(zi, yi, ci, xi):
        return {"sp": ((zi % 4) * 4 + yi % 4) * 2 + ci, "tp": xi % 4}

    sister = device(z, y, 1 - core, x)
    right, left, across = (device(z, y, core, x + d) for d in (1, 3, 2))
    yup, ydown = device(z, y + 1, core, x), device(z, y + 3, core, x)
    zup, zdown = device(z + 1, y, core, x), device(z + 3, y, core, x)
    later, earlier = {"sp": (sp + 1) % 32, "tp": x}, {"sp": (sp + 31) % 32, "tp": x}

    loads = []

    def load(src, dst):
        copy = pltpu.make_async_copy(src, dst, local.at[len(loads)])
        copy.start()
        loads.append(copy)
        return copy

    kv_copy = load(kv_h, kvv.at[:, pl.ds(WINDOW, 1024), :])
    q_copy = load(q_h, qv)
    ow_copy = load(ow_h, oww.at[0])
    up_copy = load(up_h, upw.at[z, y, core])
    raw_copy = load(dn_h.at[pl.ds(aligned(core, 1024), 1024)], raw.at[0])
    res_copy = load(res_h, resv)

    barrier = pltpu.get_barrier_semaphore()
    far = {"sp": (sp + 31 + 2 * core) % 32, "tp": x}
    friends = (sister, right, left, across, yup, ydown, zup, zdown, far)
    for friend in friends:
        pl.semaphore_signal(barrier, inc=1, device_id=friend, device_id_type=MESH)
    pl.semaphore_wait(barrier, len(friends))

    links = Links(send, recv)
    halo = [links.take() for _ in range(2)]
    links.start(
        kv_h.at[:, pl.ds(1024 - WINDOW, WINDOW), :], kvv.at[:, pl.ds(0, WINDOW), :], halo[0], later
    )
    links.start(
        kv_h.at[:, pl.ds(0, WINDOW), :], kvv.at[:, pl.ds(1024 + WINDOW, WINDOW), :], halo[1], earlier
    )

    seed = [links.take() for _ in range(3)]
    seeds = ((right, 3), (left, 1), (across, 2))
    for ident, (target, place) in zip(seed, seeds):
        links.start(ow_h.at[z, y, core], oww.at[place, z, y, core], ident, target)

    def ow_part(half, flip):
        def part_at(one, two, ci, sub):
            zi, yi = (two, one) if flip else (one, two)
            at, wide = half * 1024, 1024
            if sub is not None:
                at, wide = at + sub * 512, 512
            return oww.at[pl.ds(1, 3), zi, yi, ci, :, pl.ds(at, wide)]

        return part_at

    def up_part(half, flip):
        def part_at(one, two, ci, sub):
            zi, yi = (two, one) if flip else (one, two)
            span = pl.ds(0, 64) if sub is None else pl.ds(sub * 32, 32)
            return upw.at[zi, yi, ci, span, pl.ds(half * 1024, 1024)]

        return part_at

    def dn_part(half, flip):
        def part_at(one, two, ci, sub):
            zi, yi = (two, one) if flip else (one, two)
            at, tall = half * 512, 512
            if sub is not None:
                at, tall = at + sub * 256, 256
            span = pl.ds(pl.multiple_of(ci * 1024 + at, 256), tall)
            lanes = ALL if isinstance(yi, slice) else pl.ds(aligned(yi, 128), 128)
            return dnw.at[zi, span, lanes]

        return part_at

    def spread(make):
        return (
            Spread(links, make(0, False), z, y, core, (zup, zdown, yup, ydown), sister),
            Spread(links, make(1, True), y, z, core, (yup, ydown, zup, zdown), sister),
        )

    outs, ups, downs = spread(ow_part), spread(up_part), spread(dn_part)

    def run(pair, step):
        for one in pair:
            getattr(one, f"step{step}")()

    swap = links.take()
    links.start(dn_h.at[pl.ds(aligned(1 - core, 1024), 1024)], raw.at[1], swap, sister)

    for ident, (target, place) in zip(seed, seeds):
        links.arrived(oww.at[place, z, y, core], ident, target)
    run(outs, 1)
    up_copy.wait()
    run(ups, 1)

    def build_slab():
        raw_copy.wait()
        links.arrived(raw.at[1], swap, sister)

        def body(i, carry):
            span = pl.ds(aligned(i, 128), 128)
            mine, other = raw[0, span, :], raw[1, span, :]
            first = core == 0
            slab[span, 0:64] = jnp.where(first, mine, other)
            slab[span, 64:128] = jnp.where(first, other, mine)
            there = pl.ds(pl.multiple_of(core * 1024 + i * 128, 128), 128)
            dnw[z, there, pl.ds(aligned(y, 128), 128)] = slab[span, :]
            return carry

        lax.fori_loop(0, 8, body, 0)

    q_copy.wait()
    kv_copy.wait()
    span = BLOCK + 2 * WINDOW
    iota_r = lax.broadcasted_iota(jnp.int32, (BLOCK, span), 0)
    iota_c = lax.broadcasted_iota(jnp.int32, (BLOCK, span), 1)

    def block_copy(index, half, step, target):
        return pltpu.make_async_remote_copy(
            src_ref=att.at[index],
            dst_ref=attr.at[half, :, pl.ds(aligned(3 - step, 512), 512)],
            send_sem=asend.at[half, step],
            recv_sem=arecv.at[half, step],
            device_id=target,
            device_id_type=MESH,
        )

    events = {
        2: lambda: run(outs + ups, 2),
        3: build_slab,
        4: lambda: run(outs, 3),
        6: lambda: run(downs, 1),
    }

    def attend(index, carry):
        half, step = index // 4, index % 4
        owner = (x + 1 + step) % 4
        block = 2 * owner + half

        @pl.when(block == 0)
        def _():
            links.arrived(kvv.at[:, pl.ds(0, WINDOW), :], halo[0], later)

        @pl.when(block == 7)
        def _():
            links.arrived(kvv.at[:, pl.ds(1024 + WINDOW, WINDOW), :], halo[1], earlier)

        begin = aligned(block, BLOCK)
        pos = iota_c + (sp * 1024 + block * BLOCK - WINDOW)
        gap = iota_c - iota_r
        valid = (gap >= 0) & (gap <= 2 * WINDOW) & (pos >= 0) & (pos < total)
        for kv in range(4):
            lanes = slice(kv * HEAD_DIM, (kv + 1) * HEAD_DIM)
            keys = kvv[0, pl.ds(begin, span), lanes]
            values = kvv[1, pl.ds(begin, span), lanes]
            for sub in range(2):
                head = kv * 2 + sub
                mine = slice(head * HEAD_DIM, (head + 1) * HEAD_DIM)
                query = qv[pl.ds(begin, BLOCK), mine]
                scores = lax.dot_general(
                    query, keys, (((1,), (1,)), ((), ())), preferred_element_type=F32
                ) * HEAD_DIM ** (-0.5)
                scores = jnp.where(valid, scores, -jnp.inf)
                sink = sink_ref[head]
                top = jnp.maximum(jnp.max(scores, axis=-1, keepdims=True), sink)
                expd = jnp.exp(scores - top)
                denom = jnp.sum(expd, axis=-1, keepdims=True) + jnp.exp(sink - top)
                weights = (expd * (1.0 / denom)).astype(BF16)
                mixed = jnp.dot(weights, values, preferred_element_type=F32)
                att[index, :, mine] = mixed.astype(BF16)

        @pl.when(step < 3)
        def _():
            block_copy(index, half, step, {"sp": sp, "tp": owner}).start()

        @pl.when(step == 3)
        def _():
            attr[half, :, 0:512] = att[index]

        for when, event in events.items():
            pl.when(index == when)(event)
        return carry

    lax.fori_loop(0, 8, attend, 0)

    def peer(step):
        return (right, across, left)[step]

    gather = [[links.take() for _ in range(6)] for _ in range(2)]
    low, high = pl.ds(0, 64), pl.ds(64, 64)

    def project(half):
        for step in range(3):
            block_copy(4 * half + step, half, step, peer(step)).wait_recv()

        def body(n, carry):
            cols = pl.ds(aligned(n, 256), 256)
            weight = oww[:, :, :, :, :, cols].reshape(2048, 256)
            term = jnp.dot(attr[half], weight, preferred_element_type=F32)
            pre[:, cols] = term + resv[half * 128 : half * 128 + 128, cols].astype(F32)
            return carry

        lax.fori_loop(0, 8, body, 0)

        def norm(i, carry):
            some = pl.ds(aligned(i, 32), 32)
            rows[half, 0, some, :] = norm_rows(pre[some, :], g1_ref[...], b1_ref[...])
            return carry

        lax.fori_loop(0, 4, norm, 0)
        ids = gather[half]
        links.start(rows.at[half, 0, low], rows.at[half, 3, low], ids[0], right)
        links.start(rows.at[half, 0, high], rows.at[half, 1, high], ids[1], left)
        links.start(rows.at[half, 0, high], rows.at[half, 3, high], ids[2], right)
        links.start(rows.at[half, 0, low], rows.at[half, 1, low], ids[3], left)

    def pass_on(half):
        ids = gather[half]
        links.arrived(rows.at[half, 3, low], ids[0], right)
        links.start(rows.at[half, 3, low], rows.at[half, 2, low], ids[4], right)
        links.arrived(rows.at[half, 1, high], ids[1], left)
        links.start(rows.at[half, 1, high], rows.at[half, 2, high], ids[5], left)

    def gathered(half):
        ids = gather[half]
        links.arrived(rows.at[half, 3, high], ids[2], right)
        links.arrived(rows.at[half, 1, low], ids[3], left)
        links.arrived(rows.at[half, 2, low], ids[4], right)
        links.arrived(rows.at[half, 2, high], ids[5], left)

    def up_project(half):
        def body(n, carry):
            cols = pl.ds(aligned(n, 256), 256)
            weight = upw[:, :, :, :, cols].reshape(2048, 256)
            hidden = jnp.dot(
                rows[half].reshape(512, 2048), weight, preferred_element_type=F32
            )
            act[:, cols] = jnp.square(jnp.maximum(hidden, 0.0)).astype(BF16)
            return carry

        lax.fori_loop(0, 8, body, 0)

    scatter = [[links.take() for _ in range(6)] for _ in range(2)]

    def down_project(half):
        def body(n, carry):
            cols = pl.ds(aligned(n, 256), 256)
            weight = dnw[n // 2, :, pl.ds(aligned(n % 2, 256), 256)]
            term = jnp.dot(act[...], weight, preferred_element_type=F32)
            own[half, :, cols] = term[0:128]
            for r in range(1, 4):
                part[half, r - 1, :, cols] = term[r * 128 : r * 128 + 128].astype(BF16)
            return carry

        lax.fori_loop(0, 8, body, 0)
        ids = scatter[half]
        links.start(part.at[half, 1, low], rin.at[half, 0], ids[0], right)
        links.start(part.at[half, 1, high], rin.at[half, 1], ids[1], left)
        links.start(part.at[half, 0, high], rfin.at[half, 0, high], ids[2], right)
        links.start(part.at[half, 2, low], rfin.at[half, 1, low], ids[3], left)

    def join(half):
        ids = scatter[half]
        for side, (target, index, at) in enumerate(((right, 0, 0), (left, 2, 64))):
            links.arrived(rin.at[half, side], ids[side], target)
            span = pl.ds(at, 64)
            part[half, index, span, :] = (
                part[half, index, span, :].astype(F32) + rin[half, side].astype(F32)
            ).astype(BF16)
            links.start(
                part.at[half, index, span], rfin.at[half, side, span], ids[4 + side], target
            )

    stores = []

    def final(half):
        ids = scatter[half]
        links.arrived(rfin.at[half, 0, high], ids[2], right)
        links.arrived(rfin.at[half, 1, low], ids[3], left)
        links.arrived(rfin.at[half, 0, low], ids[4], right)
        links.arrived(rfin.at[half, 1, high], ids[5], left)

        def norm(i, carry):
            some = pl.ds(aligned(i, 32), 32)
            value = rows[half, 0, some, :].astype(F32) + own[half, some, :]
            value = value + rfin[half, 0, some, :].astype(F32)
            value = value + rfin[half, 1, some, :].astype(F32)
            outv[half, some, :] = norm_rows(value, g2_ref[...], b2_ref[...])
            return carry

        lax.fori_loop(0, 4, norm, 0)
        copy = pltpu.make_async_copy(
            outv.at[half], out_h.at[pl.ds(half * 128, 128)], local.at[6 + half]
        )
        copy.start()
        stores.append(copy)

    run(outs, 4)
    run(ups, 3)
    run(downs, 2)
    run(outs, 5)
    run(outs, 6)
    ow_copy.wait()
    res_copy.wait()
    project(0)
    project(1)
    run(ups, 4)
    run(downs, 3)
    pass_on(0)
    run(ups, 5)
    run(ups, 6)
    gathered(0)
    up_project(0)
    run(downs, 4)
    pass_on(1)
    run(downs, 5)
    run(downs, 6)
    down_project(0)
    gathered(1)
    up_project(1)
    join(0)
    down_project(1)
    final(0)
    join(1)
    final(1)
    links.finish()
    for half in range(2):
        for step in range(3):
            block_copy(4 * half + step, half, step, peer(step)).wait_send()
    for copy in stores:
        copy.wait()


def on_device(res, q, kv, sink, ow, g1, b1, up, dn, g2, b2):
    total = q.shape[0] * lax.axis_size("sp")
    hbm = pl.BlockSpec(memory_space=pl.ANY)
    vmem = pl.BlockSpec(memory_space=pltpu.VMEM)
    smem = pl.BlockSpec(memory_space=pltpu.SMEM)
    return pl.pallas_call(
        functools.partial(layer_kernel, total),
        in_specs=[hbm, hbm, hbm, smem, hbm, vmem, vmem, hbm, hbm, vmem, vmem],
        out_specs=hbm,
        out_shape=jax.ShapeDtypeStruct((256, 2048), BF16),
        scratch_shapes=[
            pltpu.VMEM((1024, 512), BF16),
            pltpu.VMEM((2, 1024 + 2 * WINDOW, 256), BF16),
            pltpu.VMEM((8, 128, 512), BF16),
            pltpu.VMEM((2, 128, 2048), BF16),
            pltpu.VMEM((256, 2048), BF16),
            pltpu.VMEM((4, 4, 4, 2, 16, 2048), BF16),
            pltpu.VMEM((4, 4, 2, 64, 2048), BF16),
            pltpu.VMEM((4, 2048, 512), BF16),
            pltpu.VMEM((2, 1024, 64), BF16),
            pltpu.VMEM((1024, 128), BF16),
            pltpu.VMEM((2, 4, 128, 2048), BF16),
            pltpu.VMEM((512, 2048), BF16),
            pltpu.VMEM((128, 2048), F32),
            pltpu.VMEM((2, 3, 128, 2048), BF16),
            pltpu.VMEM((2, 128, 2048), F32),
            pltpu.VMEM((2, 2, 64, 2048), BF16),
            pltpu.VMEM((2, 2, 128, 2048), BF16),
            pltpu.VMEM((2, 128, 2048), BF16),
            pltpu.SemaphoreType.DMA((8,)),
            pltpu.SemaphoreType.DMA((128,)),
            pltpu.SemaphoreType.DMA((128,)),
            pltpu.SemaphoreType.DMA((2, 3)),
            pltpu.SemaphoreType.DMA((2, 3)),
        ],
        compiler_params=pltpu.CompilerParams(
            collective_id=0, has_side_effects=True, vmem_limit_bytes=62 * 2**20
        ),
        cost_estimate=pl.CostEstimate(
            flops=2 * 10**10, bytes_accessed=24 * 2**20, transcendentals=4 * 10**6
        ),
        name="layer",
    )(
        res, q, kv, sink, ow.reshape(4, 4, 2, 16, 2048), g1.reshape(1, -1), b1.reshape(1, -1),
        up, dn, g2.reshape(1, -1), b2.reshape(1, -1),
    )


def solution(mesh):
    return jax.shard_map(
        on_device,
        mesh=mesh,
        in_specs=(
            P(("sp", "tp"), None),
            P("sp", "tp"),
            P(None, "sp", "tp"),
            P("tp"),
            P("tp", None),
            P(),
            P(),
            P("sp", "tp"),
            P("tp", "sp"),
            P(),
            P(),
        ),
        out_specs=P(("sp", "tp"), None),
        check_vma=False,
    )
```

profile of v0, /device:TPU:1, one launch (start us, length us, event | category | flops | bytes accessed | tf_op | source)
XLA Modules:
  0.0 148.8 jit_solution(1208209718464995832)
XLA Ops:
  0.0 2.0 %copy.12.dn_h = bf16[2048,64]{1,0:T(8,128)(2,1)} copy(bf16[2048,64]{0,1:T(8,128)(2,1)} %param.19) | data formatting | bytes 524288 | tf_op args[8]
  2.0 144.6 %layer.1 = bf16[256,2048]{1,0:T(8,128)(2,1)} custom-call(bf16[256,2048]{1,0:T(8,128)(2,1)} %res_h.1, bf16[1024,512]{1,0:T(8,128)(2,1)} %q_h.1, bf16[2,1024,256]{2,1,0:T(8,128)(2,1)} %kv_h.1, f32[8]{0:T(128)} %sink_ref.1, bf16[4,4,2,16,2048]{4,3,2,1,0:T(8,128)(2,1)} %bitcast.5, f32[1,2048]{1,0:T(1,128)} %bitcast.6, f32[1,2048]{1,0:T(1,128)} %bitcast.7, ...), custom_call_target="tpu_custom_call" | custom-call | flops 20000000000 | bytes 25165824 | tf_op jit(solution)/shard_map/layer/pallas_call | solution.py:469
  146.5 2.3 %copy.14 = bf16[256,2048]{1,0:T(8,128)(2,1)} copy(bf16[256,2048]{1,0:T(8,128)(2,1)} %layer.1) | data formatting | bytes 2097152
where the time goes:
time: 149 us
  Pallas kernels  145 us (97%)
  local copies, waits for them, and re-layouts  4.26 us (3%)
    pallas_call x1, Pallas kernels, on_device(): pl.pallas_call(functools.partial(layer_kernel, total), in_specs=[hbm, hbm...  145 us
    unnamed x2, local copies, waits for them, and re-layouts  4.26 us

commit v1 on v0

--- a/solution.py
+++ b/solution.py
@@ -10,6 +10,7 @@
 HEAD_DIM = 64
 WINDOW = 128
 BLOCK = 128
+XPART = 512
 MESH = pl.DeviceIdType.MESH
 F32 = jnp.float32
 BF16 = jnp.bfloat16
@@ -52,10 +53,12 @@
     def arrived(self, dst, ident, target):
         self.copy(dst, dst, ident, target).wait_recv()
 
-    def finish(self):
-        for again, ident, target in self.started:
+    def finish(self, keep=0):
+        count = len(self.started) - keep
+        for again, ident, target in self.started[:count]:
             src = again()
             self.copy(src, src, ident, target).wait_send()
+        self.started = self.started[count:]
 
 
 class Spread:
@@ -70,11 +73,15 @@
     def at(self, one, two, sub=None, core=None):
         return self.part(one, two, self.core if core is None else core, sub)
 
-    def push(self, ident, target, one, two, sub=None, source=None):
+    def push(self, ident, target, one, two, sub=None):
         place = self.at(one, two, sub)
-        again = (lambda: self.at(one, two, sub)) if source is None else (lambda: source)
-        src = place if source is None else source
-        self.links.start(src, place, self.ids[ident], target, again)
+        self.links.start(place, place, self.ids[ident], target, lambda: self.at(one, two, sub))
+
+    def share(self, ident, two):
+        for one in range(4):
+            place = self.at(one, two)
+            self.links.copy(place, place, self.ids[ident], self.sister).start()
+        self.links.started.append((lambda: self.at(ALL, two), self.ids[ident], self.sister))
 
     def pull(self, ident, target, one, two, sub=None, core=None):
         self.links.arrived(self.at(one, two, sub, core), self.ids[ident], target)
@@ -96,7 +103,7 @@
         self.pull(3, self.down1, across, self.own2, 1)
         self.push(4, self.up2, ALL, self.own2)
         self.push(5, self.down2, ALL, self.own2)
-        self.push(8, self.sister, ALL, self.own2)
+        self.share(8, self.own2)
 
     def step4(self):
         before, after, _ = self.near2
@@ -104,14 +111,14 @@
         self.push(6, self.up2, ALL, before, 0)
         self.pull(5, self.down2, ALL, after)
         self.push(7, self.down2, ALL, after, 1)
-        self.push(9, self.sister, ALL, before)
-        self.push(10, self.sister, ALL, after)
+        self.share(9, before)
+        self.share(10, after)
 
     def step5(self):
         across = self.near2[2]
         self.pull(6, self.up2, ALL, across, 0)
         self.pull(7, self.down2, ALL, across, 1)
-        self.push(11, self.sister, ALL, across)
+        self.share(11, across)
 
     def step6(self):
         for place, ident in zip([self.own2] + self.near2, (8, 9, 10, 11)):
@@ -119,8 +126,8 @@
 
 
 def layer_kernel(
-    total, res_h, q_h, kv_h, sink_ref, ow_h, g1_ref, b1_ref, up_h, dn_h, g2_ref, b2_ref, out_h,
-    qv, kvv, att, attr, resv, oww, upw, dnw, raw, slab, rows, act, pre, part, own, rin, rfin, outv,
+    total, res_h, q_h, kv_h, sink_ref, ow_h, g1_ref, b1_ref, up_h, dn_h, g2_ref, b2_ref, out_ref,
+    qv, kvv, att, attr, resv, oww, upw, dnw, rows, act, pre, part, own, rin, rfin, bias, scores, weights, scale,
     local, send, recv, asend, arecv,
 ):
     sp, x = lax.axis_index("sp"), lax.axis_index("tp")
@@ -148,7 +155,7 @@
     q_copy = load(q_h, qv)
     ow_copy = load(ow_h, oww.at[0])
     up_copy = load(up_h, upw.at[z, y, core])
-    raw_copy = load(dn_h.at[pl.ds(aligned(core, 1024), 1024)], raw.at[0])
+    dn_copy = load(dn_h, dnw.at[z, y, core])
     res_copy = load(res_h, resv)
 
     barrier = pltpu.get_barrier_semaphore()
@@ -156,7 +163,8 @@
     friends = (sister, right, left, across, yup, ydown, zup, zdown, far)
     for friend in friends:
         pl.semaphore_signal(barrier, inc=1, device_id=friend, device_id_type=MESH)
-    pl.semaphore_wait(barrier, len(friends))
+    with jax.named_scope("barrier"):
+        pl.semaphore_wait(barrier, len(friends))
 
     links = Links(send, recv)
     halo = [links.take() for _ in range(2)]
@@ -169,38 +177,64 @@
 
     seed = [links.take() for _ in range(3)]
     seeds = ((right, 3), (left, 1), (across, 2))
+    body_cols = pl.ds(XPART, 2048 - XPART)
     for ident, (target, place) in zip(seed, seeds):
-        links.start(ow_h.at[z, y, core], oww.at[place, z, y, core], ident, target)
+        src = ow_h.at[z, y, core, :, body_cols]
+        links.start(src, oww.at[place, z, y, core, :, body_cols], ident, target)
+    xids = [links.take() for _ in range(7)]
+
+    def xpart(place, ci, zs=ALL):
+        return oww.at[place, zs, :, ci, :, pl.ds(0, XPART)]
+
+    def xstart():
+        src = ow_h.at[:, :, core, :, pl.ds(0, XPART)]
+        links.start(src, xpart(3, core), xids[0], right)
+        links.start(src, xpart(1, core), xids[1], left)
+
+    def xpass():
+        links.arrived(xpart(3, core), xids[0], right)
+        near = xpart(3, core, pl.ds(0, 2))
+        again = lambda place, zs=ALL: lambda: xpart(place, core, zs)
+        links.start(near, xpart(2, core, pl.ds(0, 2)), xids[2], right, again(3, pl.ds(0, 2)))
+        links.arrived(xpart(1, core), xids[1], left)
+        near = xpart(1, core, pl.ds(2, 2))
+        links.start(near, xpart(2, core, pl.ds(2, 2)), xids[3], left, again(1, pl.ds(2, 2)))
+        links.start(xpart(3, core), xpart(3, core), xids[4], sister, again(3))
+        links.start(xpart(1, core), xpart(1, core), xids[5], sister, again(1))
+
+    def xshare():
+        links.arrived(xpart(2, core, pl.ds(0, 2)), xids[2], right)
+        links.arrived(xpart(2, core, pl.ds(2, 2)), xids[3], left)
+        links.start(xpart(2, core), xpart(2, core), xids[6], sister)
+
+    def xdone():
+        for place, ident in ((3, 4), (1, 5), (2, 6)):
+            links.arrived(xpart(place, 1 - core), xids[ident], sister)
+
+    xstart()
 
     def ow_part(half, flip):
         def part_at(one, two, ci, sub):
             zi, yi = (two, one) if flip else (one, two)
-            at, wide = half * 1024, 1024
+            wide = (2048 - XPART) // 2
+            at = XPART + half * wide
             if sub is not None:
-                at, wide = at + sub * 512, 512
+                wide = wide // 2
+                at = at + sub * wide
             return oww.at[pl.ds(1, 3), zi, yi, ci, :, pl.ds(at, wide)]
 
         return part_at
 
-    def up_part(half, flip):
-        def part_at(one, two, ci, sub):
-            zi, yi = (two, one) if flip else (one, two)
-            span = pl.ds(0, 64) if sub is None else pl.ds(sub * 32, 32)
-            return upw.at[zi, yi, ci, span, pl.ds(half * 1024, 1024)]
-
-        return part_at
-
-    def dn_part(half, flip):
-        def part_at(one, two, ci, sub):
-            zi, yi = (two, one) if flip else (one, two)
-            at, tall = half * 512, 512
-            if sub is not None:
-                at, tall = at + sub * 256, 256
-            span = pl.ds(pl.multiple_of(ci * 1024 + at, 256), tall)
-            lanes = ALL if isinstance(yi, slice) else pl.ds(aligned(yi, 128), 128)
-            return dnw.at[zi, span, lanes]
-
-        return part_at
+    def wide_part(buffer):
+        def make(half, flip):
+            def part_at(one, two, ci, sub):
+                zi, yi = (two, one) if flip else (one, two)
+                span = pl.ds(0, 64) if sub is None else pl.ds(sub * 32, 32)
+                return buffer.at[zi, yi, ci, span, pl.ds(half * 1024, 1024)]
+
+            return part_at
+
+        return make
 
     def spread(make):
         return (
@@ -208,37 +242,22 @@
             Spread(links, make(1, True), y, z, core, (yup, ydown, zup, zdown), sister),
         )
 
-    outs, ups, downs = spread(ow_part), spread(up_part), spread(dn_part)
-
-    def run(pair, step):
-        for one in pair:
-            getattr(one, f"step{step}")()
-
-    swap = links.take()
-    links.start(dn_h.at[pl.ds(aligned(1 - core, 1024), 1024)], raw.at[1], swap, sister)
-
-    for ident, (target, place) in zip(seed, seeds):
-        links.arrived(oww.at[place, z, y, core], ident, target)
-    run(outs, 1)
+    outs, ups, downs = spread(ow_part), spread(wide_part(upw)), spread(wide_part(dnw))
+
+    def run(name, pair, step):
+        with jax.named_scope(f"{name}{step}"):
+            for one in pair:
+                getattr(one, f"step{step}")()
+
+    def seeded():
+        with jax.named_scope("seed"):
+            for ident, (target, place) in zip(seed, seeds):
+                links.arrived(oww.at[place, z, y, core, :, body_cols], ident, target)
+        run("outs", outs, 1)
+
+    seeded()
     up_copy.wait()
-    run(ups, 1)
-
-    def build_slab():
-        raw_copy.wait()
-        links.arrived(raw.at[1], swap, sister)
-
-        def body(i, carry):
-            span = pl.ds(aligned(i, 128), 128)
-            mine, other = raw[0, span, :], raw[1, span, :]
-            first = core == 0
-            slab[span, 0:64] = jnp.where(first, mine, other)
-            slab[span, 64:128] = jnp.where(first, other, mine)
-            there = pl.ds(pl.multiple_of(core * 1024 + i * 128, 128), 128)
-            dnw[z, there, pl.ds(aligned(y, 128), 128)] = slab[span, :]
-            return carry
-
-        lax.fori_loop(0, 8, body, 0)
-
+    dn_copy.wait()
     q_copy.wait()
     kv_copy.wait()
     span = BLOCK + 2 * WINDOW
@@ -256,10 +275,10 @@
         )
 
     events = {
-        2: lambda: run(outs + ups, 2),
-        3: build_slab,
-        4: lambda: run(outs, 3),
-        6: lambda: run(downs, 1),
+        1: lambda: (run("outs", outs, 2), run("ups", ups, 1))[1],
+        3: lambda: run("outs", outs, 3),
+        4: xpass,
+        5: lambda: (run("ups", ups, 2), run("downs", downs, 1))[1],
     }
 
     def attend(index, carry):
@@ -279,25 +298,36 @@
         pos = iota_c + (sp * 1024 + block * BLOCK - WINDOW)
         gap = iota_c - iota_r
         valid = (gap >= 0) & (gap <= 2 * WINDOW) & (pos >= 0) & (pos < total)
+        bias[...] = jnp.where(valid, 0.0, -jnp.inf)
         for kv in range(4):
             lanes = slice(kv * HEAD_DIM, (kv + 1) * HEAD_DIM)
             keys = kvv[0, pl.ds(begin, span), lanes]
+            pair = [
+                qv[pl.ds(begin, BLOCK), slice(h * HEAD_DIM, (h + 1) * HEAD_DIM)]
+                for h in (2 * kv, 2 * kv + 1)
+            ]
+            query = jnp.concatenate(pair, axis=0) * jnp.asarray(HEAD_DIM ** (-0.5), BF16)
+            scores[kv] = lax.dot_general(
+                query, keys, (((1,), (1,)), ((), ())), preferred_element_type=F32
+            )
+        for head in range(8):
+            rows_of = slice((head % 2) * BLOCK, (head % 2 + 1) * BLOCK)
+            score = scores[head // 2, rows_of] + bias[...]
+            sink = sink_ref[head]
+            top = jnp.maximum(jnp.max(score, axis=-1, keepdims=True), sink)
+            expd = jnp.exp(score - top)
+            denom = jnp.sum(expd, axis=-1, keepdims=True) + jnp.exp(sink - top)
+            weights[head // 2, rows_of] = expd.astype(BF16)
+            scale[head // 2, rows_of] = jnp.broadcast_to(1.0 / denom, (BLOCK, HEAD_DIM))
+        for kv in range(4):
+            lanes = slice(kv * HEAD_DIM, (kv + 1) * HEAD_DIM)
             values = kvv[1, pl.ds(begin, span), lanes]
+            mixed = jnp.dot(weights[kv], values, preferred_element_type=F32) * scale[kv]
             for sub in range(2):
-                head = kv * 2 + sub
-                mine = slice(head * HEAD_DIM, (head + 1) * HEAD_DIM)
-                query = qv[pl.ds(begin, BLOCK), mine]
-                scores = lax.dot_general(
-                    query, keys, (((1,), (1,)), ((), ())), preferred_element_type=F32
-                ) * HEAD_DIM ** (-0.5)
-                scores = jnp.where(valid, scores, -jnp.inf)
-                sink = sink_ref[head]
-                top = jnp.maximum(jnp.max(scores, axis=-1, keepdims=True), sink)
-                expd = jnp.exp(scores - top)
-                denom = jnp.sum(expd, axis=-1, keepdims=True) + jnp.exp(sink - top)
-                weights = (expd * (1.0 / denom)).astype(BF16)
-                mixed = jnp.dot(weights, values, preferred_element_type=F32)
-                att[index, :, mine] = mixed.astype(BF16)
+                head = 2 * kv + sub
+                att[index, :, head * HEAD_DIM : (head + 1) * HEAD_DIM] = mixed[
+                    sub * BLOCK : (sub + 1) * BLOCK
+                ].astype(BF16)
 
         @pl.when(step < 3)
         def _():
@@ -311,7 +341,8 @@
             pl.when(index == when)(event)
         return carry
 
-    lax.fori_loop(0, 8, attend, 0)
+    with jax.named_scope("attend"):
+        lax.fori_loop(0, 8, attend, 0)
 
     def peer(step):
         return (right, across, left)[step]
@@ -319,25 +350,30 @@
     gather = [[links.take() for _ in range(6)] for _ in range(2)]
     low, high = pl.ds(0, 64), pl.ds(64, 64)
 
-    def project(half):
-        for step in range(3):
-            block_copy(4 * half + step, half, step, peer(step)).wait_recv()
+    def project(_):
+        for half in range(2):
+            for step in range(3):
+                block_copy(4 * half + step, half, step, peer(step)).wait_recv()
 
         def body(n, carry):
             cols = pl.ds(aligned(n, 256), 256)
             weight = oww[:, :, :, :, :, cols].reshape(2048, 256)
-            term = jnp.dot(attr[half], weight, preferred_element_type=F32)
-            pre[:, cols] = term + resv[half * 128 : half * 128 + 128, cols].astype(F32)
+            term = jnp.dot(attr[...].reshape(256, 2048), weight, preferred_element_type=F32)
+            pre[:, cols] = term + resv[:, cols].astype(F32)
             return carry
 
-        lax.fori_loop(0, 8, body, 0)
-
+        lax.fori_loop(0, 8, body, 0, unroll=4)
+
+    def norm_first(half):
         def norm(i, carry):
             some = pl.ds(aligned(i, 32), 32)
-            rows[half, 0, some, :] = norm_rows(pre[some, :], g1_ref[...], b1_ref[...])
+            there = pl.ds(pl.multiple_of(half * 128 + i * 32, 32), 32)
+            rows[half, 0, some, :] = norm_rows(pre[there, :], g1_ref[...], b1_ref[...])
             return carry
 
         lax.fori_loop(0, 4, norm, 0)
+
+    def offer(half):
         ids = gather[half]
         links.start(rows.at[half, 0, low], rows.at[half, 3, low], ids[0], right)
         links.start(rows.at[half, 0, high], rows.at[half, 1, high], ids[1], left)
@@ -368,25 +404,41 @@
             act[:, cols] = jnp.square(jnp.maximum(hidden, 0.0)).astype(BF16)
             return carry
 
-        lax.fori_loop(0, 8, body, 0)
+        lax.fori_loop(0, 8, body, 0, unroll=4)
+
+    def scoped(name, phase, half):
+        with jax.named_scope(f"{name}{half}"):
+            phase(half)
 
     scatter = [[links.take() for _ in range(6)] for _ in range(2)]
 
     def down_project(half):
+        def product(n, some):
+            weight = dnw[n // 2, pl.ds((n % 2) * 2, 2)].reshape(256, 2048)
+            return lax.dot_general(some, weight, (((1,), (1,)), ((), ())), preferred_element_type=F32)
+
         def body(n, carry):
             cols = pl.ds(aligned(n, 256), 256)
-            weight = dnw[n // 2, :, pl.ds(aligned(n % 2, 256), 256)]
-            term = jnp.dot(act[...], weight, preferred_element_type=F32)
-            own[half, :, cols] = term[0:128]
-            for r in range(1, 4):
-                part[half, r - 1, :, cols] = term[r * 128 : r * 128 + 128].astype(BF16)
+            term = product(n, act[128:384, :])
+            part[half, 0, :, cols] = term[0:128].astype(BF16)
+            part[half, 1, :, cols] = term[128:256].astype(BF16)
             return carry
 
-        lax.fori_loop(0, 8, body, 0)
+        lax.fori_loop(0, 8, body, 0, unroll=4)
         ids = scatter[half]
         links.start(part.at[half, 1, low], rin.at[half, 0], ids[0], right)
         links.start(part.at[half, 1, high], rin.at[half, 1], ids[1], left)
         links.start(part.at[half, 0, high], rfin.at[half, 0, high], ids[2], right)
+
+        def body(n, carry):
+            cols = pl.ds(aligned(n, 256), 256)
+            some = jnp.concatenate([act[384:512, :], act[0:128, :]], axis=0)
+            term = product(n, some)
+            part[half, 2, :, cols] = term[0:128].astype(BF16)
+            own[half, :, cols] = term[128:256]
+            return carry
+
+        lax.fori_loop(0, 8, body, 0, unroll=4)
         links.start(part.at[half, 2, low], rfin.at[half, 1, low], ids[3], left)
 
     def join(half):
@@ -401,8 +453,6 @@
                 part.at[half, index, span], rfin.at[half, side, span], ids[4 + side], target
             )
 
-    stores = []
-
     def final(half):
         ids = scatter[half]
         links.arrived(rfin.at[half, 0, high], ids[2], right)
@@ -415,62 +465,64 @@
             value = rows[half, 0, some, :].astype(F32) + own[half, some, :]
             value = value + rfin[half, 0, some, :].astype(F32)
             value = value + rfin[half, 1, some, :].astype(F32)
-            outv[half, some, :] = norm_rows(value, g2_ref[...], b2_ref[...])
+            there = pl.ds(pl.multiple_of(half * 128 + i * 32, 32), 32)
+            out_ref[there, :] = norm_rows(value, g2_ref[...], b2_ref[...])
             return carry
 
         lax.fori_loop(0, 4, norm, 0)
-        copy = pltpu.make_async_copy(
-            outv.at[half], out_h.at[pl.ds(half * 128, 128)], local.at[6 + half]
-        )
-        copy.start()
-        stores.append(copy)
-
-    run(outs, 4)
-    run(ups, 3)
-    run(downs, 2)
-    run(outs, 5)
-    run(outs, 6)
+
+    run("outs", outs, 4)
+    with jax.named_scope("xshare"):
+        xshare()
+    run("downs", downs, 2)
+    run("outs", outs, 5)
+    run("ups", ups, 3)
+    run("outs", outs, 6)
+    with jax.named_scope("xdone"):
+        xdone()
     ow_copy.wait()
     res_copy.wait()
-    project(0)
-    project(1)
-    run(ups, 4)
-    run(downs, 3)
-    pass_on(0)
-    run(ups, 5)
-    run(ups, 6)
-    gathered(0)
-    up_project(0)
-    run(downs, 4)
-    pass_on(1)
-    run(downs, 5)
-    run(downs, 6)
-    down_project(0)
-    gathered(1)
-    up_project(1)
-    join(0)
-    down_project(1)
-    final(0)
-    join(1)
-    final(1)
-    links.finish()
+    scoped("project", project, 0)
+    scoped("norm_first", norm_first, 0)
+    offer(0)
+    scoped("norm_first", norm_first, 1)
+    run("ups", ups, 4)
+    run("downs", downs, 3)
+    scoped("pass_on", pass_on, 0)
+    offer(1)
+    run("ups", ups, 5)
+    run("ups", ups, 6)
+    scoped("gathered", gathered, 0)
+    scoped("up_project", up_project, 0)
+    run("downs", downs, 4)
+    scoped("pass_on", pass_on, 1)
+    run("downs", downs, 5)
+    run("downs", downs, 6)
+    scoped("down_project", down_project, 0)
+    scoped("gathered", gathered, 1)
+    scoped("up_project", up_project, 1)
+    scoped("join", join, 0)
+    scoped("down_project", down_project, 1)
+    scoped("final", final, 0)
+    scoped("join", join, 1)
     for half in range(2):
         for step in range(3):
             block_copy(4 * half + step, half, step, peer(step)).wait_send()
-    for copy in stores:
-        copy.wait()
+    links.finish(2)
+    scoped("final", final, 1)
+    links.finish()
 
 
 def on_device(res, q, kv, sink, ow, g1, b1, up, dn, g2, b2):
     total = q.shape[0] * lax.axis_size("sp")
-    hbm = pl.BlockSpec(memory_space=pl.ANY)
+    hbm = pl.BlockSpec(memory_space=pltpu.HBM)
     vmem = pl.BlockSpec(memory_space=pltpu.VMEM)
     smem = pl.BlockSpec(memory_space=pltpu.SMEM)
     return pl.pallas_call(
         functools.partial(layer_kernel, total),
         in_specs=[hbm, hbm, hbm, smem, hbm, vmem, vmem, hbm, hbm, vmem, vmem],
-        out_specs=hbm,
-        out_shape=jax.ShapeDtypeStruct((256, 2048), BF16),
+        out_specs=vmem,
+        out_shape=pltpu.VMEM((256, 2048), BF16),
         scratch_shapes=[
             pltpu.VMEM((1024, 512), BF16),
             pltpu.VMEM((2, 1024 + 2 * WINDOW, 256), BF16),
@@ -479,17 +531,18 @@
             pltpu.VMEM((256, 2048), BF16),
             pltpu.VMEM((4, 4, 4, 2, 16, 2048), BF16),
             pltpu.VMEM((4, 4, 2, 64, 2048), BF16),
-            pltpu.VMEM((4, 2048, 512), BF16),
-            pltpu.VMEM((2, 1024, 64), BF16),
-            pltpu.VMEM((1024, 128), BF16),
+            pltpu.VMEM((4, 4, 2, 64, 2048), BF16),
             pltpu.VMEM((2, 4, 128, 2048), BF16),
             pltpu.VMEM((512, 2048), BF16),
-            pltpu.VMEM((128, 2048), F32),
+            pltpu.VMEM((256, 2048), F32),
             pltpu.VMEM((2, 3, 128, 2048), BF16),
             pltpu.VMEM((2, 128, 2048), F32),
             pltpu.VMEM((2, 2, 64, 2048), BF16),
             pltpu.VMEM((2, 2, 128, 2048), BF16),
-            pltpu.VMEM((2, 128, 2048), BF16),
+            pltpu.VMEM((BLOCK, BLOCK + 2 * WINDOW), F32),
+            pltpu.VMEM((4, 2 * BLOCK, BLOCK + 2 * WINDOW), F32),
+            pltpu.VMEM((4, 2 * BLOCK, BLOCK + 2 * WINDOW), BF16),
+            pltpu.VMEM((4, 2 * BLOCK, HEAD_DIM), F32),
             pltpu.SemaphoreType.DMA((8,)),
             pltpu.SemaphoreType.DMA((128,)),
             pltpu.SemaphoreType.DMA((128,)),
@@ -505,7 +558,7 @@
         name="layer",
     )(
         res, q, kv, sink, ow.reshape(4, 4, 2, 16, 2048), g1.reshape(1, -1), b1.reshape(1, -1),
-        up, dn, g2.reshape(1, -1), b2.reshape(1, -1),
+        up, dn.T, g2.reshape(1, -1), b2.reshape(1, -1),
     )
 
 

time: 149 us -> 119 us (0.80)
  Pallas kernels: 145 us -> 117 us
  local copies, waits for them, and re-layouts: 4.26 us -> 0.97 us
    pallas_call x1, Pallas kernels: 145 us -> 117 us  [on_device(): pl.pallas_call(functools.partial(layer_kernel, total), in_specs=[hbm, hbm...]
    unnamed x2 -> x1, local copies, waits for them, and re-layouts: 4.26 us -> 0.97 us
where the time goes in v1:
time: 119 us; the launch traced here: 118 us
  Pallas kernels  117 us (98%)
    pallas_call x1, Pallas kernels, on_device(): pl.pallas_call(functools.partial(layer_kernel, total), in_specs=[hbm, hbm...  117 us

profile of v1, /device:TPU:1, one launch (start us, length us, event | category | flops | bytes accessed | tf_op | source)
XLA Modules:
  0.0 118.1 jit_solution(9894773006705046336)
XLA Ops:
  0.0 117.1 %layer.1 = bf16[256,2048]{1,0:T(8,128)(2,1)S(1)} custom-call(bf16[256,2048]{1,0:T(8,128)(2,1)} %res_h.1, bf16[1024,512]{1,0:T(8,128)(2,1)} %q_h.1, bf16[2,1024,256]{2,1,0:T(8,128)(2,1)} %kv_h.1, f32[8]{0:T(128)} %sink_ref.1, bf16[4,4,2,16,2048]{4,3,2,1,0:T(8,128)(2,1)} %bitcast.6, f32[1,2048]{1,0:T(1,128)} %bitcast.8, f32[1,2048]{1,0:T(1,128)} %bitcast.9, ...), custom_call_target="tpu_custom_call" | custom-call | flops 20000000000 | bytes 25165824 | tf_op jit(solution)/shard_map/layer/pallas_call | solution.py:521
  117.2 1.0 copy.13

commit v2 on v1

--- a/solution.py
+++ b/solution.py
@@ -62,11 +62,12 @@
 
 
 class Spread:
-    def __init__(self, links, part, first, second, core, peers, sister):
+    def __init__(self, links, part, first, second, core, peers, sister, opposite=None):
         self.links, self.part, self.core, self.sister = links, part, core, sister
+        self.opposite = opposite
         self.own1, self.own2 = first, second
         self.up1, self.down1, self.up2, self.down2 = peers
-        self.ids = [links.take() for _ in range(12)]
+        self.ids = [links.take() for _ in range(14)]
         self.near1 = [(first + hop) % 4 for hop in (3, 1, 2)]
         self.near2 = [(second + hop) % 4 for hop in (3, 1, 2)]
 
@@ -89,9 +90,16 @@
     def step1(self):
         self.push(0, self.up1, self.own1, self.own2)
         self.push(1, self.down1, self.own1, self.own2)
+        if self.opposite is not None:
+            self.push(2, self.opposite, self.own1, self.own2)
 
     def step2(self):
-        before, after, _ = self.near1
+        before, after, across = self.near1
+        if self.opposite is not None:
+            self.pull(0, self.up1, before, self.own2)
+            self.pull(1, self.down1, after, self.own2)
+            self.pull(2, self.opposite, across, self.own2)
+            return
         self.pull(0, self.up1, before, self.own2)
         self.push(2, self.up1, before, self.own2, 0)
         self.pull(1, self.down1, after, self.own2)
@@ -99,28 +107,36 @@
 
     def step3(self):
         across = self.near1[2]
-        self.pull(2, self.up1, across, self.own2, 0)
-        self.pull(3, self.down1, across, self.own2, 1)
-        self.push(4, self.up2, ALL, self.own2)
-        self.push(5, self.down2, ALL, self.own2)
+        if self.opposite is None:
+            self.pull(2, self.up1, across, self.own2, 0)
+            self.pull(3, self.down1, across, self.own2, 1)
+        self.push(4, self.up2, ALL, self.own2, 0)
+        self.push(5, self.down2, ALL, self.own2, 1)
+        self.push(12, self.up2, ALL, self.own2, 1)
+        self.push(13, self.down2, ALL, self.own2, 0)
         self.share(8, self.own2)
 
     def step4(self):
         before, after, _ = self.near2
-        self.pull(4, self.up2, ALL, before)
+        self.pull(4, self.up2, ALL, before, 0)
         self.push(6, self.up2, ALL, before, 0)
-        self.pull(5, self.down2, ALL, after)
+        self.pull(5, self.down2, ALL, after, 1)
         self.push(7, self.down2, ALL, after, 1)
+
+    def step5(self):
+        before, after, _ = self.near2
+        self.pull(12, self.up2, ALL, before, 1)
         self.share(9, before)
+        self.pull(13, self.down2, ALL, after, 0)
         self.share(10, after)
 
-    def step5(self):
+    def step6(self):
         across = self.near2[2]
         self.pull(6, self.up2, ALL, across, 0)
         self.pull(7, self.down2, ALL, across, 1)
         self.share(11, across)
 
-    def step6(self):
+    def step7(self):
         for place, ident in zip([self.own2] + self.near2, (8, 9, 10, 11)):
             self.pull(ident, self.sister, ALL, place, None, 1 - self.core)
 
@@ -151,16 +167,17 @@
         loads.append(copy)
         return copy
 
+    ow_copy = load(ow_h, oww.at[0])
     kv_copy = load(kv_h, kvv.at[:, pl.ds(WINDOW, 1024), :])
     q_copy = load(q_h, qv)
-    ow_copy = load(ow_h, oww.at[0])
     up_copy = load(up_h, upw.at[z, y, core])
     dn_copy = load(dn_h, dnw.at[z, y, core])
     res_copy = load(res_h, resv)
 
     barrier = pltpu.get_barrier_semaphore()
     far = {"sp": (sp + 31 + 2 * core) % 32, "tp": x}
-    friends = (sister, right, left, across, yup, ydown, zup, zdown, far)
+    zfar, yfar = device(z + 2, y, core, x), device(z, y + 2, core, x)
+    friends = (sister, right, left, across, yup, ydown, zup, zdown, far, zfar, yfar)
     for friend in friends:
         pl.semaphore_signal(barrier, inc=1, device_id=friend, device_id_type=MESH)
     with jax.named_scope("barrier"):
@@ -168,18 +185,13 @@
 
     links = Links(send, recv)
     halo = [links.take() for _ in range(2)]
-    links.start(
-        kv_h.at[:, pl.ds(1024 - WINDOW, WINDOW), :], kvv.at[:, pl.ds(0, WINDOW), :], halo[0], later
-    )
-    links.start(
-        kv_h.at[:, pl.ds(0, WINDOW), :], kvv.at[:, pl.ds(1024 + WINDOW, WINDOW), :], halo[1], earlier
-    )
 
     seed = [links.take() for _ in range(3)]
     seeds = ((right, 3), (left, 1), (across, 2))
     body_cols = pl.ds(XPART, 2048 - XPART)
+    ow_copy.wait()
     for ident, (target, place) in zip(seed, seeds):
-        src = ow_h.at[z, y, core, :, body_cols]
+        src = oww.at[0, z, y, core, :, body_cols]
         links.start(src, oww.at[place, z, y, core, :, body_cols], ident, target)
     xids = [links.take() for _ in range(7)]
 
@@ -187,7 +199,7 @@
         return oww.at[place, zs, :, ci, :, pl.ds(0, XPART)]
 
     def xstart():
-        src = ow_h.at[:, :, core, :, pl.ds(0, XPART)]
+        src = xpart(0, core)
         links.start(src, xpart(3, core), xids[0], right)
         links.start(src, xpart(1, core), xids[1], left)
 
@@ -211,6 +223,10 @@
         for place, ident in ((3, 4), (1, 5), (2, 6)):
             links.arrived(xpart(place, 1 - core), xids[ident], sister)
 
+    kv_copy.wait()
+    last, start = pl.ds(1024, WINDOW), pl.ds(WINDOW, WINDOW)
+    links.start(kvv.at[:, last, :], kvv.at[:, pl.ds(0, WINDOW), :], halo[0], later)
+    links.start(kvv.at[:, start, :], kvv.at[:, pl.ds(1024 + WINDOW, WINDOW), :], halo[1], earlier)
     xstart()
 
     def ow_part(half, flip):
@@ -219,8 +235,8 @@
             wide = (2048 - XPART) // 2
             at = XPART + half * wide
             if sub is not None:
-                wide = wide // 2
-                at = at + sub * wide
+                first = (wide + 128) // 256 * 128
+                at, wide = at + sub * first, wide - first if sub else first
             return oww.at[pl.ds(1, 3), zi, yi, ci, :, pl.ds(at, wide)]
 
         return part_at
@@ -236,13 +252,13 @@
 
         return make
 
-    def spread(make):
+    def spread(make, zfar=None, yfar=None):
         return (
-            Spread(links, make(0, False), z, y, core, (zup, zdown, yup, ydown), sister),
-            Spread(links, make(1, True), y, z, core, (yup, ydown, zup, zdown), sister),
+            Spread(links, make(0, False), z, y, core, (zup, zdown, yup, ydown), sister, zfar),
+            Spread(links, make(1, True), y, z, core, (yup, ydown, zup, zdown), sister, yfar),
         )
 
-    outs, ups, downs = spread(ow_part), spread(wide_part(upw)), spread(wide_part(dnw))
+    outs, ups, downs = spread(ow_part, zfar, yfar), spread(wide_part(upw)), spread(wide_part(dnw))
 
     def run(name, pair, step):
         with jax.named_scope(f"{name}{step}"):
@@ -259,7 +275,6 @@
     up_copy.wait()
     dn_copy.wait()
     q_copy.wait()
-    kv_copy.wait()
     span = BLOCK + 2 * WINDOW
     iota_r = lax.broadcasted_iota(jnp.int32, (BLOCK, span), 0)
     iota_c = lax.broadcasted_iota(jnp.int32, (BLOCK, span), 1)
@@ -275,10 +290,8 @@
         )
 
     events = {
-        1: lambda: (run("outs", outs, 2), run("ups", ups, 1))[1],
-        3: lambda: run("outs", outs, 3),
+        1: lambda: (run("outs", outs, 2), run("outs", outs, 3), run("ups", ups, 1))[2],
         4: xpass,
-        5: lambda: (run("ups", ups, 2), run("downs", downs, 1))[1],
     }
 
     def attend(index, carry):
@@ -472,32 +485,36 @@
         lax.fori_loop(0, 4, norm, 0)
 
     run("outs", outs, 4)
+    run("ups", ups, 2)
+    run("downs", downs, 1)
     with jax.named_scope("xshare"):
         xshare()
-    run("downs", downs, 2)
     run("outs", outs, 5)
+    run("outs", outs, 6)
     run("ups", ups, 3)
-    run("outs", outs, 6)
+    run("outs", outs, 7)
     with jax.named_scope("xdone"):
         xdone()
-    ow_copy.wait()
     res_copy.wait()
     scoped("project", project, 0)
     scoped("norm_first", norm_first, 0)
     offer(0)
     scoped("norm_first", norm_first, 1)
+    run("downs", downs, 2)
     run("ups", ups, 4)
-    run("downs", downs, 3)
     scoped("pass_on", pass_on, 0)
     offer(1)
     run("ups", ups, 5)
+    run("downs", downs, 3)
     run("ups", ups, 6)
+    run("ups", ups, 7)
     scoped("gathered", gathered, 0)
+    run("downs", downs, 4)
     scoped("up_project", up_project, 0)
-    run("downs", downs, 4)
+    run("downs", downs, 5)
     scoped("pass_on", pass_on, 1)
-    run("downs", downs, 5)
     run("downs", downs, 6)
+    run("downs", downs, 7)
     scoped("down_project", down_project, 0)
     scoped("gathered", gathered, 1)
     scoped("up_project", up_project, 1)

time: 119 us -> 114 us (0.958)
  Pallas kernels: 117 us -> 113 us
    pallas_call x1, Pallas kernels: 117 us -> 113 us  [on_device(): pl.pallas_call(functools.partial(layer_kernel, total), in_specs=[hbm, hbm...]
where the time goes in v2:
time: 114 us
  Pallas kernels  113 us (99%)
    pallas_call x1, Pallas kernels, on_device(): pl.pallas_call(functools.partial(layer_kernel, total), in_specs=[hbm, hbm...  113 us

profile of v2, /device:TPU:1, one launch (start us, length us, event | category | flops | bytes accessed | tf_op | source)
XLA Modules:
  0.0 114.0 jit_solution(2658094958249179922)
XLA Ops:
  0.0 113.0 %layer.1 = bf16[256,2048]{1,0:T(8,128)(2,1)S(1)} custom-call(bf16[256,2048]{1,0:T(8,128)(2,1)} %res_h.1, bf16[1024,512]{1,0:T(8,128)(2,1)} %q_h.1, bf16[2,1024,256]{2,1,0:T(8,128)(2,1)} %kv_h.1, f32[8]{0:T(128)} %sink_ref.1, bf16[4,4,2,16,2048]{4,3,2,1,0:T(8,128)(2,1)} %bitcast.6, f32[1,2048]{1,0:T(1,128)} %bitcast.8, f32[1,2048]{1,0:T(1,128)} %bitcast.9, ...), custom_call_target="tpu_custom_call" | custom-call | flops 20000000000 | bytes 25165824 | tf_op jit(solution)/shard_map/layer/pallas_call | solution.py:538
  113.0 1.0 copy.13

commit v3 on v2

--- a/solution.py
+++ b/solution.py
@@ -10,7 +10,8 @@
 HEAD_DIM = 64
 WINDOW = 128
 BLOCK = 128
-XPART = 512
+XPART = 768
+SENDS = 40
 MESH = pl.DeviceIdType.MESH
 F32 = jnp.float32
 BF16 = jnp.bfloat16
@@ -31,43 +32,54 @@
 class Links:
     def __init__(self, send, recv):
         self.send, self.recv, self.count, self.started = send, recv, 0, []
+        self.turn = 0
 
     def take(self):
         self.count += 1
         return self.count - 1
 
-    def copy(self, src, dst, ident, target):
+    def copy(self, src, dst, ident, target, slot=0):
         return pltpu.make_async_remote_copy(
             src_ref=src,
             dst_ref=dst,
-            send_sem=self.send.at[ident],
+            send_sem=self.send.at[slot],
             recv_sem=self.recv.at[ident],
             device_id=target,
             device_id_type=MESH,
         )
 
+    def slot(self):
+        slot = self.turn % SENDS
+        self.turn += 1
+        if self.turn > SENDS:
+            self.left(self.started.pop(0))
+        return slot
+
+    def left(self, entry):
+        again, ident, target, slot = entry
+        src = again()
+        self.copy(src, src, ident, target, slot).wait_send()
+
     def start(self, src, dst, ident, target, again=None):
-        self.copy(src, dst, ident, target).start()
-        self.started.append((again or (lambda: src), ident, target))
+        slot = self.slot()
+        self.copy(src, dst, ident, target, slot).start()
+        self.started.append((again or (lambda: src), ident, target, slot))
 
     def arrived(self, dst, ident, target):
         self.copy(dst, dst, ident, target).wait_recv()
 
     def finish(self, keep=0):
-        count = len(self.started) - keep
-        for again, ident, target in self.started[:count]:
-            src = again()
-            self.copy(src, src, ident, target).wait_send()
-        self.started = self.started[count:]
+        while len(self.started) > keep:
+            self.left(self.started.pop(0))
 
 
 class Spread:
-    def __init__(self, links, part, first, second, core, peers, sister, opposite=None):
+    def __init__(self, links, part, first, second, core, peers, sister, common, opposite=None):
         self.links, self.part, self.core, self.sister = links, part, core, sister
-        self.opposite = opposite
+        self.opposite, self.common = opposite, common
         self.own1, self.own2 = first, second
         self.up1, self.down1, self.up2, self.down2 = peers
-        self.ids = [links.take() for _ in range(14)]
+        self.ids = [links.take() for _ in range(10)]
         self.near1 = [(first + hop) % 4 for hop in (3, 1, 2)]
         self.near2 = [(second + hop) % 4 for hop in (3, 1, 2)]
 
@@ -78,11 +90,13 @@
         place = self.at(one, two, sub)
         self.links.start(place, place, self.ids[ident], target, lambda: self.at(one, two, sub))
 
-    def share(self, ident, two):
+    def share(self, two, sub=None, far=False):
+        slot, ident = self.links.slot(), self.common[far]
         for one in range(4):
-            place = self.at(one, two)
-            self.links.copy(place, place, self.ids[ident], self.sister).start()
-        self.links.started.append((lambda: self.at(ALL, two), self.ids[ident], self.sister))
+            place = self.at(one, two, sub)
+            self.links.copy(place, place, ident, self.sister, slot).start()
+        entry = (lambda: self.at(ALL, two, sub), ident, self.sister, slot)
+        self.links.started.append(entry)
 
     def pull(self, ident, target, one, two, sub=None, core=None):
         self.links.arrived(self.at(one, two, sub, core), self.ids[ident], target)
@@ -112,9 +126,9 @@
             self.pull(3, self.down1, across, self.own2, 1)
         self.push(4, self.up2, ALL, self.own2, 0)
         self.push(5, self.down2, ALL, self.own2, 1)
-        self.push(12, self.up2, ALL, self.own2, 1)
-        self.push(13, self.down2, ALL, self.own2, 0)
-        self.share(8, self.own2)
+        self.push(8, self.up2, ALL, self.own2, 1)
+        self.push(9, self.down2, ALL, self.own2, 0)
+        self.share(self.own2)
 
     def step4(self):
         before, after, _ = self.near2
@@ -122,29 +136,27 @@
         self.push(6, self.up2, ALL, before, 0)
         self.pull(5, self.down2, ALL, after, 1)
         self.push(7, self.down2, ALL, after, 1)
+        self.share(before, 0)
+        self.share(after, 1)
 
     def step5(self):
         before, after, _ = self.near2
-        self.pull(12, self.up2, ALL, before, 1)
-        self.share(9, before)
-        self.pull(13, self.down2, ALL, after, 0)
-        self.share(10, after)
+        self.pull(8, self.up2, ALL, before, 1)
+        self.share(before, 1)
+        self.pull(9, self.down2, ALL, after, 0)
+        self.share(after, 0)
 
     def step6(self):
         across = self.near2[2]
         self.pull(6, self.up2, ALL, across, 0)
         self.pull(7, self.down2, ALL, across, 1)
-        self.share(11, across)
-
-    def step7(self):
-        for place, ident in zip([self.own2] + self.near2, (8, 9, 10, 11)):
-            self.pull(ident, self.sister, ALL, place, None, 1 - self.core)
+        self.share(across, far=True)
 
 
 def layer_kernel(
-    total, res_h, q_h, kv_h, sink_ref, ow_h, g1_ref, b1_ref, up_h, dn_h, g2_ref, b2_ref, out_ref,
+    total, res_h, q_h, kv_h, sink_h, ow_h, g1_h, b1_h, up_h, dn_h, g2_h, b2_h, out_ref,
     qv, kvv, att, attr, resv, oww, upw, dnw, rows, act, pre, part, own, rin, rfin, bias, scores, weights, scale,
-    local, send, recv, asend, arecv,
+    sink_ref, g1_ref, b1_ref, g2_ref, b2_ref, local, send, recv, asend, arecv,
 ):
     sp, x = lax.axis_index("sp"), lax.axis_index("tp")
     core, chip = sp % 2, sp // 2
@@ -172,7 +184,10 @@
     q_copy = load(q_h, qv)
     up_copy = load(up_h, upw.at[z, y, core])
     dn_copy = load(dn_h, dnw.at[z, y, core])
+    sink_copy = load(sink_h, sink_ref)
     res_copy = load(res_h, resv)
+    pairs = ((g1_h, g1_ref), (b1_h, b1_ref), (g2_h, g2_ref), (b2_h, b2_ref))
+    norm_copies = [load(src, dst) for src, dst in pairs]
 
     barrier = pltpu.get_barrier_semaphore()
     far = {"sp": (sp + 31 + 2 * core) % 32, "tp": x}
@@ -186,14 +201,14 @@
     links = Links(send, recv)
     halo = [links.take() for _ in range(2)]
 
-    seed = [links.take() for _ in range(3)]
+    seed = links.take()
     seeds = ((right, 3), (left, 1), (across, 2))
     body_cols = pl.ds(XPART, 2048 - XPART)
     ow_copy.wait()
-    for ident, (target, place) in zip(seed, seeds):
+    for target, place in seeds:
         src = oww.at[0, z, y, core, :, body_cols]
-        links.start(src, oww.at[place, z, y, core, :, body_cols], ident, target)
-    xids = [links.take() for _ in range(7)]
+        links.start(src, oww.at[place, z, y, core, :, body_cols], seed, target)
+    xids = [links.take() for _ in range(4)]
 
     def xpart(place, ci, zs=ALL):
         return oww.at[place, zs, :, ci, :, pl.ds(0, XPART)]
@@ -211,17 +226,13 @@
         links.arrived(xpart(1, core), xids[1], left)
         near = xpart(1, core, pl.ds(2, 2))
         links.start(near, xpart(2, core, pl.ds(2, 2)), xids[3], left, again(1, pl.ds(2, 2)))
-        links.start(xpart(3, core), xpart(3, core), xids[4], sister, again(3))
-        links.start(xpart(1, core), xpart(1, core), xids[5], sister, again(1))
+        links.start(xpart(3, core), xpart(3, core), ow_all, sister, again(3))
+        links.start(xpart(1, core), xpart(1, core), ow_all, sister, again(1))
 
     def xshare():
         links.arrived(xpart(2, core, pl.ds(0, 2)), xids[2], right)
         links.arrived(xpart(2, core, pl.ds(2, 2)), xids[3], left)
-        links.start(xpart(2, core), xpart(2, core), xids[6], sister)
-
-    def xdone():
-        for place, ident in ((3, 4), (1, 5), (2, 6)):
-            links.arrived(xpart(place, 1 - core), xids[ident], sister)
+        links.start(xpart(2, core), xpart(2, core), ow_all, sister)
 
     kv_copy.wait()
     last, start = pl.ds(1024, WINDOW), pl.ds(WINDOW, WINDOW)
@@ -252,13 +263,16 @@
 
         return make
 
-    def spread(make, zfar=None, yfar=None):
+    def spread(make, common, zfar=None, yfar=None):
         return (
-            Spread(links, make(0, False), z, y, core, (zup, zdown, yup, ydown), sister, zfar),
-            Spread(links, make(1, True), y, z, core, (yup, ydown, zup, zdown), sister, yfar),
+            Spread(links, make(0, False), z, y, core, (zup, zdown, yup, ydown), sister, common, zfar),
+            Spread(links, make(1, True), y, z, core, (yup, ydown, zup, zdown), sister, common, yfar),
         )
 
-    outs, ups, downs = spread(ow_part, zfar, yfar), spread(wide_part(upw)), spread(wide_part(dnw))
+    ow_all, up_all, dn_near, dn_far = (links.take() for _ in range(4))
+    outs = spread(ow_part, (ow_all, ow_all), zfar, yfar)
+    ups = spread(wide_part(upw), (up_all, up_all))
+    downs = spread(wide_part(dnw), (dn_near, dn_far))
 
     def run(name, pair, step):
         with jax.named_scope(f"{name}{step}"):
@@ -267,14 +281,19 @@
 
     def seeded():
         with jax.named_scope("seed"):
-            for ident, (target, place) in zip(seed, seeds):
-                links.arrived(oww.at[place, z, y, core, :, body_cols], ident, target)
+            links.arrived(oww.at[pl.ds(1, 3), z, y, core, :, body_cols], seed, right)
         run("outs", outs, 1)
 
+    def complete(name, half, ident):
+        with jax.named_scope(f"{name}7"):
+            links.arrived(half, ident, sister)
+
+    up_copy.wait()
+    run("ups", ups, 1)
+    dn_copy.wait()
     seeded()
-    up_copy.wait()
-    dn_copy.wait()
     q_copy.wait()
+    sink_copy.wait()
     span = BLOCK + 2 * WINDOW
     iota_r = lax.broadcasted_iota(jnp.int32, (BLOCK, span), 0)
     iota_c = lax.broadcasted_iota(jnp.int32, (BLOCK, span), 1)
@@ -290,8 +309,10 @@
         )
 
     events = {
-        1: lambda: (run("outs", outs, 2), run("outs", outs, 3), run("ups", ups, 1))[2],
+        1: lambda: (run("outs", outs, 2), run("outs", outs, 3), run("ups", ups, 2))[2],
+        3: lambda: run("downs", downs, 1),
         4: xpass,
+        6: lambda: run("outs", outs, 4),
     }
 
     def attend(index, carry):
@@ -360,19 +381,19 @@
     def peer(step):
         return (right, across, left)[step]
 
-    gather = [[links.take() for _ in range(6)] for _ in range(2)]
+    gather = [[links.take() for _ in range(3)] for _ in range(2)]
     low, high = pl.ds(0, 64), pl.ds(64, 64)
 
-    def project(_):
-        for half in range(2):
-            for step in range(3):
-                block_copy(4 * half + step, half, step, peer(step)).wait_recv()
+    def project(half):
+        for step in range(3):
+            block_copy(4 * half + step, half, step, peer(step)).wait_recv()
 
         def body(n, carry):
             cols = pl.ds(aligned(n, 256), 256)
             weight = oww[:, :, :, :, :, cols].reshape(2048, 256)
-            term = jnp.dot(attr[...].reshape(256, 2048), weight, preferred_element_type=F32)
-            pre[:, cols] = term + resv[:, cols].astype(F32)
+            term = jnp.dot(attr[half], weight, preferred_element_type=F32)
+            there = slice(half * 128, half * 128 + 128)
+            pre[there, cols] = term + resv[there, cols].astype(F32)
             return carry
 
         lax.fori_loop(0, 8, body, 0, unroll=4)
@@ -391,21 +412,17 @@
         links.start(rows.at[half, 0, low], rows.at[half, 3, low], ids[0], right)
         links.start(rows.at[half, 0, high], rows.at[half, 1, high], ids[1], left)
         links.start(rows.at[half, 0, high], rows.at[half, 3, high], ids[2], right)
-        links.start(rows.at[half, 0, low], rows.at[half, 1, low], ids[3], left)
+        links.start(rows.at[half, 0, low], rows.at[half, 1, low], ids[2], left)
 
     def pass_on(half):
         ids = gather[half]
         links.arrived(rows.at[half, 3, low], ids[0], right)
-        links.start(rows.at[half, 3, low], rows.at[half, 2, low], ids[4], right)
+        links.start(rows.at[half, 3, low], rows.at[half, 2, low], ids[2], right)
         links.arrived(rows.at[half, 1, high], ids[1], left)
-        links.start(rows.at[half, 1, high], rows.at[half, 2, high], ids[5], left)
+        links.start(rows.at[half, 1, high], rows.at[half, 2, high], ids[2], left)
 
     def gathered(half):
-        ids = gather[half]
-        links.arrived(rows.at[half, 3, high], ids[2], right)
-        links.arrived(rows.at[half, 1, low], ids[3], left)
-        links.arrived(rows.at[half, 2, low], ids[4], right)
-        links.arrived(rows.at[half, 2, high], ids[5], left)
+        links.arrived(rows.at[half, pl.ds(1, 2)], gather[half][2], right)
 
     def up_project(half):
         def body(n, carry):
@@ -423,7 +440,7 @@
         with jax.named_scope(f"{name}{half}"):
             phase(half)
 
-    scatter = [[links.take() for _ in range(6)] for _ in range(2)]
+    scatter = [[links.take() for _ in range(3)] for _ in range(2)]
 
     def down_project(half):
         def product(n, some):
@@ -437,7 +454,21 @@
             part[half, 1, :, cols] = term[128:256].astype(BF16)
             return carry
 
-        lax.fori_loop(0, 8, body, 0, unroll=4)
+        def tile(n):
+            body(n, 0)
+
+        if half:
+            lax.fori_loop(0, 8, body, 0, unroll=4)
+        else:
+            there = (y + 2) % 4 // 2
+            for hop in (0, 1, 3):
+                tile((z + hop) % 4 * 2 + 1 - there)
+            run("downs", downs, 6)
+            complete("downs", dnw.at[0, :, 1 - core], dn_far)
+            for hop in (0, 1, 3):
+                tile((z + hop) % 4 * 2 + there)
+            for pair in range(2):
+                tile((z + 2) % 4 * 2 + pair)
         ids = scatter[half]
         links.start(part.at[half, 1, low], rin.at[half, 0], ids[0], right)
         links.start(part.at[half, 1, high], rin.at[half, 1], ids[1], left)
@@ -452,7 +483,7 @@
             return carry
 
         lax.fori_loop(0, 8, body, 0, unroll=4)
-        links.start(part.at[half, 2, low], rfin.at[half, 1, low], ids[3], left)
+        links.start(part.at[half, 2, low], rfin.at[half, 1, low], ids[2], left)
 
     def join(half):
         ids = scatter[half]
@@ -463,15 +494,11 @@
                 part[half, index, span, :].astype(F32) + rin[half, side].astype(F32)
             ).astype(BF16)
             links.start(
-                part.at[half, index, span], rfin.at[half, side, span], ids[4 + side], target
+                part.at[half, index, span], rfin.at[half, side, span], ids[2], target
             )
 
     def final(half):
-        ids = scatter[half]
-        links.arrived(rfin.at[half, 0, high], ids[2], right)
-        links.arrived(rfin.at[half, 1, low], ids[3], left)
-        links.arrived(rfin.at[half, 0, low], ids[4], right)
-        links.arrived(rfin.at[half, 1, high], ids[5], left)
+        links.arrived(rfin.at[half], scatter[half][2], right)
 
         def norm(i, carry):
             some = pl.ds(aligned(i, 32), 32)
@@ -484,37 +511,34 @@
 
         lax.fori_loop(0, 4, norm, 0)
 
-    run("outs", outs, 4)
-    run("ups", ups, 2)
-    run("downs", downs, 1)
+    run("outs", outs, 5)
+    run("downs", downs, 2)
+    run("ups", ups, 3)
+    run("outs", outs, 6)
     with jax.named_scope("xshare"):
         xshare()
-    run("outs", outs, 5)
-    run("outs", outs, 6)
-    run("ups", ups, 3)
-    run("outs", outs, 7)
-    with jax.named_scope("xdone"):
-        xdone()
+    complete("outs", oww.at[pl.ds(1, 3), :, :, 1 - core], ow_all)
     res_copy.wait()
+    for copy in norm_copies:
+        copy.wait()
     scoped("project", project, 0)
     scoped("norm_first", norm_first, 0)
     offer(0)
+    scoped("project", project, 1)
     scoped("norm_first", norm_first, 1)
-    run("downs", downs, 2)
     run("ups", ups, 4)
     scoped("pass_on", pass_on, 0)
     offer(1)
     run("ups", ups, 5)
     run("downs", downs, 3)
     run("ups", ups, 6)
-    run("ups", ups, 7)
+    complete("ups", upw.at[:, :, 1 - core], up_all)
     scoped("gathered", gathered, 0)
     run("downs", downs, 4)
     scoped("up_project", up_project, 0)
     run("downs", downs, 5)
     scoped("pass_on", pass_on, 1)
-    run("downs", downs, 6)
-    run("downs", downs, 7)
+    complete("near", dnw.at[pl.ds(0, 3), :, 1 - core], dn_near)
     scoped("down_project", down_project, 0)
     scoped("gathered", gathered, 1)
     scoped("up_project", up_project, 1)
@@ -527,17 +551,17 @@
             block_copy(4 * half + step, half, step, peer(step)).wait_send()
     links.finish(2)
     scoped("final", final, 1)
-    links.finish()
+    with jax.named_scope("finish"):
+        links.finish()
 
 
 def on_device(res, q, kv, sink, ow, g1, b1, up, dn, g2, b2):
     total = q.shape[0] * lax.axis_size("sp")
     hbm = pl.BlockSpec(memory_space=pltpu.HBM)
     vmem = pl.BlockSpec(memory_space=pltpu.VMEM)
-    smem = pl.BlockSpec(memory_space=pltpu.SMEM)
     return pl.pallas_call(
         functools.partial(layer_kernel, total),
-        in_specs=[hbm, hbm, hbm, smem, hbm, vmem, vmem, hbm, hbm, vmem, vmem],
+        in_specs=[hbm] * 11,
         out_specs=vmem,
         out_shape=pltpu.VMEM((256, 2048), BF16),
         scratch_shapes=[
@@ -560,9 +584,14 @@
             pltpu.VMEM((4, 2 * BLOCK, BLOCK + 2 * WINDOW), F32),
             pltpu.VMEM((4, 2 * BLOCK, BLOCK + 2 * WINDOW), BF16),
             pltpu.VMEM((4, 2 * BLOCK, HEAD_DIM), F32),
-            pltpu.SemaphoreType.DMA((8,)),
-            pltpu.SemaphoreType.DMA((128,)),
-            pltpu.SemaphoreType.DMA((128,)),
+            pltpu.SMEM((8,), F32),
+            pltpu.VMEM((1, 2048), F32),
+            pltpu.VMEM((1, 2048), F32),
+            pltpu.VMEM((1, 2048), F32),
+            pltpu.VMEM((1, 2048), F32),
+            pltpu.SemaphoreType.DMA((12,)),
+            pltpu.SemaphoreType.DMA((SENDS,)),
+            pltpu.SemaphoreType.DMA((83,)),
             pltpu.SemaphoreType.DMA((2, 3)),
             pltpu.SemaphoreType.DMA((2, 3)),
         ],

time: 114 us -> 110 us (0.965)
  Pallas kernels: 113 us -> 109 us
    pallas_call x1, Pallas kernels: 113 us -> 109 us  [on_device(): pl.pallas_call(functools.partial(layer_kernel, total), in_specs=[hbm] * 1...]
where the time goes in v3:
time: 110 us
  Pallas kernels  109 us (99%)
    pallas_call x1, Pallas kernels, on_device(): pl.pallas_call(functools.partial(layer_kernel, total), in_specs=[hbm] * 1...  109 us

profile of v3, /device:TPU:1, one launch (start us, length us, event | category | flops | bytes accessed | tf_op | source)
XLA Modules:
  0.0 109.6 jit_solution(5356595142138266420)
XLA Ops:
  0.0 108.6 %layer.1 = bf16[256,2048]{1,0:T(8,128)(2,1)S(1)} custom-call(bf16[256,2048]{1,0:T(8,128)(2,1)} %res_h.1, bf16[1024,512]{1,0:T(8,128)(2,1)} %q_h.1, bf16[2,1024,256]{2,1,0:T(8,128)(2,1)} %kv_h.1, f32[8]{0:T(128)} %sink_h.1, bf16[4,4,2,16,2048]{4,3,2,1,0:T(8,128)(2,1)} %bitcast.6, f32[1,2048]{1,0:T(1,128)} %bitcast.8, f32[1,2048]{1,0:T(1,128)} %bitcast.9, ...), custom_call_target="tpu_custom_call" | custom-call | flops 20000000000 | bytes 25165824 | tf_op jit(solution)/shard_map/layer/pallas_call | solution.py:562
  108.7 1.0 copy.13

commit v4 on v3

--- a/solution.py
+++ b/solution.py
@@ -310,9 +310,9 @@
 
     events = {
         1: lambda: (run("outs", outs, 2), run("outs", outs, 3), run("ups", ups, 2))[2],
-        3: lambda: run("downs", downs, 1),
-        4: xpass,
-        6: lambda: run("outs", outs, 4),
+        3: xpass,
+        5: lambda: (run("outs", outs, 4), run("downs", downs, 1))[1],
+        6: lambda: run("ups", ups, 3),
     }
 
     def attend(index, carry):
@@ -405,7 +405,7 @@
             rows[half, 0, some, :] = norm_rows(pre[there, :], g1_ref[...], b1_ref[...])
             return carry
 
-        lax.fori_loop(0, 4, norm, 0)
+        lax.fori_loop(0, 4, norm, 0, unroll=2)
 
     def offer(half):
         ids = gather[half]
@@ -509,11 +509,9 @@
             out_ref[there, :] = norm_rows(value, g2_ref[...], b2_ref[...])
             return carry
 
-        lax.fori_loop(0, 4, norm, 0)
+        lax.fori_loop(0, 4, norm, 0, unroll=2)
 
     run("outs", outs, 5)
-    run("downs", downs, 2)
-    run("ups", ups, 3)
     run("outs", outs, 6)
     with jax.named_scope("xshare"):
         xshare()
@@ -526,6 +524,7 @@
     offer(0)
     scoped("project", project, 1)
     scoped("norm_first", norm_first, 1)
+    run("downs", downs, 2)
     run("ups", ups, 4)
     scoped("pass_on", pass_on, 0)
     offer(1)

time: 110 us -> 109 us (level)
  no operation moved by 1% of the time
where the time goes in v4:
time: 109 us
  Pallas kernels  108 us (99%)
    pallas_call x1, Pallas kernels, on_device(): pl.pallas_call(functools.partial(layer_kernel, total), in_specs=[hbm] * 1...  108 us

profile of v4, /device:TPU:1, one launch (start us, length us, event | category | flops | bytes accessed | tf_op | source)
XLA Modules:
  0.0 108.7 jit_solution(7032126570227876010)
XLA Ops:
  0.0 107.7 %layer.1 = bf16[256,2048]{1,0:T(8,128)(2,1)S(1)} custom-call(bf16[256,2048]{1,0:T(8,128)(2,1)} %res_h.1, bf16[1024,512]{1,0:T(8,128)(2,1)} %q_h.1, bf16[2,1024,256]{2,1,0:T(8,128)(2,1)} %kv_h.1, f32[8]{0:T(128)} %sink_h.1, bf16[4,4,2,16,2048]{4,3,2,1,0:T(8,128)(2,1)} %bitcast.6, f32[1,2048]{1,0:T(1,128)} %bitcast.8, f32[1,2048]{1,0:T(1,128)} %bitcast.9, ...), custom_call_target="tpu_custom_call" | custom-call | flops 20000000000 | bytes 25165824 | tf_op jit(solution)/shard_map/layer/pallas_call | solution.py:561
  107.7 1.0 copy.13

commit v5 on v4

--- a/solution.py
+++ b/solution.py
@@ -11,7 +11,7 @@
 WINDOW = 128
 BLOCK = 128
 XPART = 768
-SENDS = 40
+SENDS = 56
 MESH = pl.DeviceIdType.MESH
 F32 = jnp.float32
 BF16 = jnp.bfloat16
@@ -447,6 +447,13 @@
             weight = dnw[n // 2, pl.ds((n % 2) * 2, 2)].reshape(256, 2048)
             return lax.dot_general(some, weight, (((1,), (1,)), ((), ())), preferred_element_type=F32)
 
+        ids = scatter[half]
+
+        def spread_out(cols):
+            links.start(part.at[half, 1, low, cols], rin.at[half, 0, :, cols], ids[0], right)
+            links.start(part.at[half, 1, high, cols], rin.at[half, 1, :, cols], ids[1], left)
+            links.start(part.at[half, 0, high, cols], rfin.at[half, 0, high, cols], ids[2], right)
+
         def body(n, carry):
             cols = pl.ds(aligned(n, 256), 256)
             term = product(n, act[128:384, :])
@@ -456,9 +463,11 @@
 
         def tile(n):
             body(n, 0)
+            spread_out(pl.ds(aligned(n, 256), 256))
 
         if half:
             lax.fori_loop(0, 8, body, 0, unroll=4)
+            spread_out(ALL)
         else:
             there = (y + 2) % 4 // 2
             for hop in (0, 1, 3):
@@ -469,11 +478,6 @@
                 tile((z + hop) % 4 * 2 + there)
             for pair in range(2):
                 tile((z + 2) % 4 * 2 + pair)
-        ids = scatter[half]
-        links.start(part.at[half, 1, low], rin.at[half, 0], ids[0], right)
-        links.start(part.at[half, 1, high], rin.at[half, 1], ids[1], left)
-        links.start(part.at[half, 0, high], rfin.at[half, 0, high], ids[2], right)
-
         def body(n, carry):
             cols = pl.ds(aligned(n, 256), 256)
             some = jnp.concatenate([act[384:512, :], act[0:128, :]], axis=0)

time: 109 us -> 107 us (0.982)
  Pallas kernels: 108 us -> 106 us
    pallas_call x1, Pallas kernels: 108 us -> 106 us  [on_device(): pl.pallas_call(functools.partial(layer_kernel, total), in_specs=[hbm] * 1...]
where the time goes in v5:
time: 107 us
  Pallas kernels  106 us (99%)
    pallas_call x1, Pallas kernels, on_device(): pl.pallas_call(functools.partial(layer_kernel, total), in_specs=[hbm] * 1...  106 us

profile of v5, /device:TPU:1, one launch (start us, length us, event | category | flops | bytes accessed | tf_op | source)
XLA Modules:
  0.0 106.9 jit_solution(8762298921203806571)
XLA Ops:
  0.0 105.9 %layer.1 = bf16[256,2048]{1,0:T(8,128)(2,1)S(1)} custom-call(bf16[256,2048]{1,0:T(8,128)(2,1)} %res_h.1, bf16[1024,512]{1,0:T(8,128)(2,1)} %q_h.1, bf16[2,1024,256]{2,1,0:T(8,128)(2,1)} %kv_h.1, f32[8]{0:T(128)} %sink_h.1, bf16[4,4,2,16,2048]{4,3,2,1,0:T(8,128)(2,1)} %bitcast.6, f32[1,2048]{1,0:T(1,128)} %bitcast.8, f32[1,2048]{1,0:T(1,128)} %bitcast.9, ...), custom_call_target="tpu_custom_call" | custom-call | flops 20000000000 | bytes 25165824 | tf_op jit(solution)/shard_map/layer/pallas_call | solution.py:565
  105.9 1.0 copy.13

commit v6 on v5

--- a/solution.py
+++ b/solution.py
@@ -79,7 +79,7 @@
         self.opposite, self.common = opposite, common
         self.own1, self.own2 = first, second
         self.up1, self.down1, self.up2, self.down2 = peers
-        self.ids = [links.take() for _ in range(10)]
+        self.ids = [links.take() for _ in range(7)]
         self.near1 = [(first + hop) % 4 for hop in (3, 1, 2)]
         self.near2 = [(second + hop) % 4 for hop in (3, 1, 2)]
 
@@ -117,39 +117,36 @@
         self.pull(0, self.up1, before, self.own2)
         self.push(2, self.up1, before, self.own2, 0)
         self.pull(1, self.down1, after, self.own2)
-        self.push(3, self.down1, after, self.own2, 1)
+        self.push(2, self.down1, after, self.own2, 1)
 
     def step3(self):
         across = self.near1[2]
         if self.opposite is None:
-            self.pull(2, self.up1, across, self.own2, 0)
-            self.pull(3, self.down1, across, self.own2, 1)
-        self.push(4, self.up2, ALL, self.own2, 0)
-        self.push(5, self.down2, ALL, self.own2, 1)
-        self.push(8, self.up2, ALL, self.own2, 1)
-        self.push(9, self.down2, ALL, self.own2, 0)
+            self.pull(2, self.up1, across, self.own2)
+        self.push(3, self.up2, ALL, self.own2, 0)
+        self.push(4, self.down2, ALL, self.own2, 1)
+        self.push(6, self.up2, ALL, self.own2, 1)
+        self.push(6, self.down2, ALL, self.own2, 0)
         self.share(self.own2)
 
     def step4(self):
         before, after, _ = self.near2
-        self.pull(4, self.up2, ALL, before, 0)
-        self.push(6, self.up2, ALL, before, 0)
-        self.pull(5, self.down2, ALL, after, 1)
-        self.push(7, self.down2, ALL, after, 1)
+        self.pull(3, self.up2, ALL, before, 0)
+        self.push(5, self.up2, ALL, before, 0)
+        self.pull(4, self.down2, ALL, after, 1)
+        self.push(5, self.down2, ALL, after, 1)
         self.share(before, 0)
         self.share(after, 1)
 
     def step5(self):
         before, after, _ = self.near2
-        self.pull(8, self.up2, ALL, before, 1)
+        self.pull(6, self.up2, ALL, before)
         self.share(before, 1)
-        self.pull(9, self.down2, ALL, after, 0)
         self.share(after, 0)
 
     def step6(self):
         across = self.near2[2]
-        self.pull(6, self.up2, ALL, across, 0)
-        self.pull(7, self.down2, ALL, across, 1)
+        self.pull(5, self.up2, ALL, across)
         self.share(across, far=True)
 
 
@@ -398,18 +395,20 @@
 
         lax.fori_loop(0, 8, body, 0, unroll=4)
 
-    def norm_first(half):
+    def norm_first(half, parts):
         def norm(i, carry):
             some = pl.ds(aligned(i, 32), 32)
             there = pl.ds(pl.multiple_of(half * 128 + i * 32, 32), 32)
             rows[half, 0, some, :] = norm_rows(pre[there, :], g1_ref[...], b1_ref[...])
             return carry
 
-        lax.fori_loop(0, 4, norm, 0, unroll=2)
+        lax.fori_loop(*parts, norm, 0, unroll=2)
 
     def offer(half):
         ids = gather[half]
+        norm_first(half, (0, 2))
         links.start(rows.at[half, 0, low], rows.at[half, 3, low], ids[0], right)
+        norm_first(half, (2, 4))
         links.start(rows.at[half, 0, high], rows.at[half, 1, high], ids[1], left)
         links.start(rows.at[half, 0, high], rows.at[half, 3, high], ids[2], right)
         links.start(rows.at[half, 0, low], rows.at[half, 1, low], ids[2], left)
@@ -524,10 +523,8 @@
     for copy in norm_copies:
         copy.wait()
     scoped("project", project, 0)
-    scoped("norm_first", norm_first, 0)
     offer(0)
     scoped("project", project, 1)
-    scoped("norm_first", norm_first, 1)
     run("downs", downs, 2)
     run("ups", ups, 4)
     scoped("pass_on", pass_on, 0)
@@ -594,7 +591,7 @@
             pltpu.VMEM((1, 2048), F32),
             pltpu.SemaphoreType.DMA((12,)),
             pltpu.SemaphoreType.DMA((SENDS,)),
-            pltpu.SemaphoreType.DMA((83,)),
+            pltpu.SemaphoreType.DMA((65,)),
             pltpu.SemaphoreType.DMA((2, 3)),
             pltpu.SemaphoreType.DMA((2, 3)),
         ],

time: 107 us -> 106 us (level)
  no operation moved by 1% of the time
where the time goes in v6:
time: 106 us
  Pallas kernels  105 us (99%)
    pallas_call x1, Pallas kernels, on_device(): pl.pallas_call(functools.partial(layer_kernel, total), in_specs=[hbm] * 1...  105 us

profile of v6, /device:TPU:1, one launch (start us, length us, event | category | flops | bytes accessed | tf_op | source)
XLA Modules:
  0.0 106.4 jit_solution(14170442826084766609)
XLA Ops:
  0.0 105.4 %layer.1 = bf16[256,2048]{1,0:T(8,128)(2,1)S(1)} custom-call(bf16[256,2048]{1,0:T(8,128)(2,1)} %res_h.1, bf16[1024,512]{1,0:T(8,128)(2,1)} %q_h.1, bf16[2,1024,256]{2,1,0:T(8,128)(2,1)} %kv_h.1, f32[8]{0:T(128)} %sink_h.1, bf16[4,4,2,16,2048]{4,3,2,1,0:T(8,128)(2,1)} %bitcast.6, f32[1,2048]{1,0:T(1,128)} %bitcast.8, f32[1,2048]{1,0:T(1,128)} %bitcast.9, ...), custom_call_target="tpu_custom_call" | custom-call | flops 20000000000 | bytes 25165824 | tf_op jit(solution)/shard_map/layer/pallas_call | solution.py:562
  105.4 1.0 copy.13
